TPU v7x, 32 devices: a whole 2x2x4 slice. The times are simulated.
32 devices in a mesh: sp: 8 (over z, y), tp: 4 (over x, core).
Axes of the slice: x: 2, y: 2, z: 4, core: 2. Of those that a mesh axis runs over, the one named last changes fastest.
Arguments:
- inputs: bfloat16 [2, 1024, 2048], P(None, 'sp'), may hold values from -6 to 6
- norm_gain: float32 [2048], replicated, may hold values from 0.1 to 1.9
- query_weight: bfloat16 [2048, 1024], P('sp', 'tp'), may hold values from -0.125 to 0.125
- key_weight: bfloat16 [2048, 256], P('sp', 'tp'), may hold values from -0.125 to 0.125
- value_weight: bfloat16 [2048, 256], P('sp', 'tp'), may hold values from -0.125 to 0.125
- query_gain: float32 [64], replicated, may hold values from 0.1 to 24
- key_gain: float32 [64], replicated, may hold values from 0.1 to 1.9
- forget_cache: float32 [2, 16, 1024], P(None, 'tp'), may hold values from -104 to 0, as said below
- rec_in_weight: bfloat16 [2048, 1024], P('sp', 'tp'), may hold values from -0.125 to 0.125
- rec_gate_weight: bfloat16 [2048, 1024], P('sp', 'tp'), may hold values from -0.125 to 0.125
- conv_weight: bfloat16 [4, 1024], P(None, 'tp'), may hold values from -3 to 3
- decay_gate_weight: bfloat16 [16, 64, 64], P('tp'), may hold values from -0.75 to 0.75
- input_gate_weight: bfloat16 [16, 64, 64], P('tp'), may hold values from -0.75 to 0.75
- decay_param: float32 [1024], P('tp'), may hold values from 4 to 16
- decay_extra: float32 [2, 1024, 1024], P(None, 'sp', 'tp'), may hold values from -2 to 0
- attn_out_gain: float32 [1024], P('tp'), may hold values from 0.1 to 1.9
- rec_out_gain: float32 [1024], P('tp'), may hold values from 0.1 to 1.9
- out_att_weight: bfloat16 [1024, 2048], P('tp'), may hold values from -0.125 to 0.125
- out_rec_weight: bfloat16 [1024, 2048], P('tp'), may hold values from -0.125 to 0.125
Outputs:
- mixed: bfloat16 [2, 1024, 2048], P(None, 'sp', 'tp')
Inputs may be any that keep to these rules, and one draw needn't show every extreme that they name: `forget_cache`: Non-increasing along the positions of each sequence and head.
All inputs are finite; a program needn't handle non-finite values.
Results may differ from a plain program's by a relative error of at most 0.012.
The roundings to bfloat16 on the way count: a program that leaves them out, or rounds other values in their place, can miss the bound.
Values may be sent and summed in bfloat16 or wider, within the bound.
A program may use at most 128 MiB of HBM per device.

v0:
```python
import jax
import jax.numpy as jnp
from jax import lax
from jax.sharding import PartitionSpec as P

D = 2048
LRU_BLOCK = 64
CONV_TAPS = 4


lru_const = 8.0
norm_eps = 1e-06


def from_behind(value, axis, steps):
    count = lax.axis_size(axis)
    leading, last = (max(0, -steps), min(count, count - steps))
    return lax.ppermute(value, axis, [(source, source + steps) for source in range(leading, last)])


def rms_scale(values, gain):
    multiplier = lax.rsqrt(jnp.mean(values * values, axis=-1, keepdims=True) + norm_eps)
    return values * multiplier * gain


def merge_state(earlier, later):
    return (earlier[0] * later[0], later[0] * earlier[1] + later[1])


def block_length(length, span):
    shards = max(length // span, 1)
    group_size = 1
    for trial_size in range(1, shards + 1):
        if shards % trial_size == 0 and trial_size * span <= 1024:
            group_size = trial_size
    sub_size = group_size * span
    if length % sub_size:
        sub_size = length
    return sub_size


def body(
    inputs,
    norm_gain,
    query_weight,
    key_weight,
    value_weight,
    query_gain,
    key_gain,
    forget_cache,
    rec_in_weight,
    rec_gate_weight,
    conv_weight,
    decay_gate_weight,
    input_gate_weight,
    decay_param,
    decay_extra,
    attn_out_gain,
    rec_out_gain,
    out_att_weight,
    out_rec_weight,
):
    seq_count, seq_span, model_width = inputs.shape
    row_count = seq_count * seq_span
    head_dim = query_gain.shape[0]
    att_local = query_weight.shape[1] // head_dim
    kv_local = key_weight.shape[1] // head_dim
    head_group = att_local // kv_local
    channels = rec_in_weight.shape[1]
    normed = rms_scale(
        inputs.reshape(row_count, model_width).astype(jnp.float32), norm_gain
    ).astype(jnp.bfloat16)
    normed_cols = normed.T
    row_contract = (((0,), (0,)), ((), ()))
    kv_cols = key_weight.shape[1]
    pieces = (
        lax.all_gather(query_weight, "sp", axis=0, tiled=True),
        lax.all_gather(key_weight, "sp", axis=0, tiled=True),
        lax.all_gather(value_weight, "sp", axis=0, tiled=True),
        lax.all_gather(rec_in_weight, "sp", axis=0, tiled=True),
        lax.all_gather(rec_gate_weight, "sp", axis=0, tiled=True),
    )
    query_proj, key_proj, value_sum, rec_in_sum, gate_proj = tuple(
        (
            lax.dot_general(
                normed_cols, weight_part, row_contract, preferred_element_type=jnp.float32
            )
            for weight_part in pieces
        )
    )
    queries = rms_scale(query_proj.reshape(row_count, att_local, head_dim), query_gain).astype(
        jnp.bfloat16
    )
    queries = queries.reshape(seq_count, seq_span, kv_local, head_group, head_dim).transpose(
        0, 2, 3, 1, 4
    )
    queries = queries.reshape(seq_count, kv_local, head_group * seq_span, head_dim)
    key_heads = rms_scale(key_proj.reshape(row_count, kv_local, head_dim), key_gain).astype(
        jnp.bfloat16
    )
    key_heads = key_heads.reshape(seq_count, seq_span, kv_cols)
    value_heads = value_sum.astype(jnp.bfloat16).reshape(seq_count, seq_span, kv_cols)
    key_value = jnp.concatenate([key_heads, value_heads], axis=2)
    my_first = lax.axis_index("sp") * seq_span
    own_gates = lax.dynamic_slice_in_dim(forget_cache, my_first, seq_span, 2)
    own_gates = own_gates.reshape(seq_count, kv_local, head_group, seq_span, 1)
    query_pos = my_first + jnp.tile(jnp.arange(seq_span, dtype=jnp.int32), head_group)
    scaling = head_dim ** (-0.5)
    start_state = (
        jnp.full((seq_count, kv_local, head_group * seq_span), -jnp.inf, jnp.float32),
        jnp.zeros((seq_count, kv_local, head_group * seq_span), jnp.float32),
        jnp.zeros((seq_count, kv_local, head_group * seq_span, head_dim), jnp.float32),
    )
    shard_part = lax.all_gather(key_value, "sp", axis=1, tiled=True)
    offset = jnp.int32(0)
    length = shard_part.shape[1]
    sub_size = block_length(length, seq_span)

    def one_step(block_index, carried_state):
        key_first = offset + block_index * sub_size

        def work(carried):
            top_score, totals, accum = carried
            block_rows = lax.dynamic_slice_in_dim(shard_part, block_index * sub_size, sub_size, 1)
            key_block = block_rows[:, :, :kv_cols].reshape(seq_count, sub_size, kv_local, head_dim)
            value_block = block_rows[:, :, kv_cols:].reshape(
                seq_count, sub_size, kv_local, head_dim
            )
            key_gates = lax.dynamic_slice_in_dim(forget_cache, key_first, sub_size, 2)
            key_gates = key_gates.reshape(seq_count, kv_local, head_group, 1, sub_size)
            scores = (
                jnp.einsum(
                    "bhqd,bkhd->bhqk", queries, key_block, preferred_element_type=jnp.float32
                )
                * scaling
            )
            scores = (
                scores.reshape(seq_count, kv_local, head_group, seq_span, sub_size)
                + own_gates
                - key_gates
            )
            scores = scores.reshape(seq_count, kv_local, head_group * seq_span, sub_size)
            visible = (
                query_pos[:, None] >= (key_first + jnp.arange(sub_size, dtype=jnp.int32))[None, :]
            )
            scores = jnp.where(visible, scores, -jnp.inf)
            new_top = jnp.maximum(top_score, jnp.max(scores, axis=-1))
            safe_top = jnp.where(jnp.isfinite(new_top), new_top, 0.0)
            weights = jnp.exp(scores - safe_top[..., None])
            fading = jnp.exp(top_score - safe_top)
            totals = totals * fading + jnp.sum(weights, axis=-1)
            accum = accum * fading[..., None] + jnp.einsum(
                "bhqk,bkhd->bhqd",
                weights.astype(jnp.bfloat16),
                value_block,
                preferred_element_type=jnp.float32,
            )
            return (new_top, totals, accum)

        return lax.cond(
            key_first < my_first + seq_span, work, lambda carried: carried, carried_state
        )

    top_score, totals, accum = lax.fori_loop(0, length // sub_size, one_step, start_state)
    attended = (accum / totals[..., None]).reshape(
        seq_count, kv_local, head_group, seq_span, head_dim
    )
    attended = attended.transpose(0, 3, 1, 2, 4).reshape(row_count, att_local, head_dim)
    att_normed = rms_scale(attended, attn_out_gain.reshape(att_local, head_dim)).astype(
        jnp.bfloat16
    )
    att_normed = att_normed.reshape(row_count, att_local * head_dim)
    rec_in = rec_in_sum.astype(jnp.bfloat16).reshape(seq_count, seq_span, channels)
    before = from_behind(rec_in[:, seq_span - (CONV_TAPS - 1) :, :], "sp", 1)
    extended = jnp.concatenate([before, rec_in], axis=1)
    conv = jnp.zeros((seq_count, seq_span, channels), jnp.float32)
    for tap in range(CONV_TAPS):
        conv = conv + extended[:, tap : tap + seq_span].astype(jnp.float32) * conv_weight[
            tap
        ].astype(jnp.float32)
    conv = conv.astype(jnp.bfloat16)
    blocks_local = decay_gate_weight.shape[0]
    grouped = conv.reshape(seq_count, seq_span, blocks_local, LRU_BLOCK)
    gate_decay = jnp.einsum(
        "bsnd,nde->bsne", grouped, decay_gate_weight, preferred_element_type=jnp.float32
    ).reshape(seq_count, seq_span, channels)
    gate_input = jnp.einsum(
        "bsnd,nde->bsne", grouped, input_gate_weight, preferred_element_type=jnp.float32
    ).reshape(seq_count, seq_span, channels)
    log_decay = (
        -lru_const * jax.nn.sigmoid(gate_decay) * jax.nn.softplus(-decay_param) + decay_extra
    )
    drive = (
        jnp.sqrt(-jnp.expm1(2.0 * log_decay))
        * jax.nn.sigmoid(gate_input)
        * conv.astype(jnp.float32)
    )
    cum_decay, local_state = lax.associative_scan(merge_state, (jnp.exp(log_decay), drive), axis=1)
    every_decay, every_state = (
        lax.all_gather(cum_decay[:, seq_span - 1][None], "sp", axis=0, tiled=True),
        lax.all_gather(local_state[:, seq_span - 1][None], "sp", axis=0, tiled=True),
    )
    prefix_decay, prefix_state = lax.associative_scan(
        merge_state, (every_decay, every_state), axis=0
    )
    position = lax.axis_index("sp")
    earlier_state = lax.dynamic_index_in_dim(
        prefix_state, jnp.maximum(position - 1, 0), 0, keepdims=False
    )
    entering = jnp.where(position > 0, earlier_state, 0.0)
    state = local_state + cum_decay * entering[:, None, :]
    gated = state * jax.nn.gelu(gate_proj.reshape(seq_count, seq_span, channels))
    rec_normed = rms_scale(
        gated.reshape(row_count, blocks_local, LRU_BLOCK),
        rec_out_gain.reshape(blocks_local, LRU_BLOCK),
    ).astype(jnp.bfloat16)
    rec_normed = rec_normed.reshape(row_count, channels)
    out_cols = D // lax.axis_size("tp")
    pieces = row_count * lax.axis_size("tp") // row_count
    terms = jnp.dot(att_normed, out_att_weight, preferred_element_type=jnp.float32) + jnp.dot(
        rec_normed, out_rec_weight, preferred_element_type=jnp.float32
    )
    mixed_cols = lax.psum_scatter(
        terms.reshape(row_count, pieces, out_cols)
        .transpose(1, 0, 2)
        .reshape(pieces * row_count, out_cols)
        .astype(jnp.bfloat16),
        "tp",
        scatter_dimension=0,
        tiled=True,
    )
    return mixed_cols.reshape(seq_count, seq_span, out_cols)


def solution(mesh):
    return jax.shard_map(
        body,
        mesh=mesh,
        in_specs=(
            P(None, "sp", None),
            P(),
            P("sp", "tp"),
            P("sp", "tp"),
            P("sp", "tp"),
            P(),
            P(),
            P(None, "tp", None),
            P("sp", "tp"),
            P("sp", "tp"),
            P(None, "tp"),
            P("tp", None, None),
            P("tp", None, None),
            P("tp"),
            P(None, "sp", "tp"),
            P("tp"),
            P("tp"),
            P("tp", None),
            P("tp", None),
        ),
        out_specs=P(None, "sp", "tp"),
        check_vma=False,
    )
```

profile of v0, /device:TPU:0, one launch (start us, length us, event | category | flops | bytes accessed | tf_op | source)
XLA Modules:
  0.0 263.9 jit_solution(10849590766930557368)
XLA Ops:
  6.5 0.7 all-gather.6.cloned.1.call-update
  7.3 0.7 all-gather.8.cloned.1.call-update
  8.1 0.7 all-gather.10.cloned.1.call-update
  8.8 0.7 fusion.67
  9.5 1.5 multiply_reduce_fusion
  11.0 1.4 slice_convert_fusion.3
  12.4 33.4 %all_gather.25 = bf16[2048,64]{0,1:T(8,128)(2,1)S(1)} all-gather(bf16[256,64]{0,1:T(8,128)(2,1)} %param.24), channel_id=1, replica_groups=mesh['sp'=8,'tp'=4] {'sp'}, dimensions={0}, use_global_device_ids=true | all-gather | bytes 294912 | tf_op jit(solution)/shard_map/all_gather | solution.py:78
  45.8 31.4 %all_gather.26 = bf16[2048,64]{0,1:T(8,128)(2,1)S(1)} all-gather(bf16[256,64]{0,1:T(8,128)(2,1)} %param.25), channel_id=1, replica_groups=mesh['sp'=8,'tp'=4] {'sp'}, dimensions={0}, use_global_device_ids=true | all-gather | bytes 294912 | tf_op jit(solution)/shard_map/all_gather | solution.py:79
  77.2 1.0 fusion.14
  79.3 29.7 %all_gather.27 = bf16[2,1024,128]{1,2,0:T(8,128)(2,1)} all-gather(bf16[2,128,128]{1,2,0:T(8,128)(2,1)S(1)} %pad_maximum_fusion.3), channel_id=1, replica_groups=mesh['sp'=8,'tp'=4] {'sp'}, dimensions={1}, use_global_device_ids=true | all-gather | bytes 589824 | tf_op jit(solution)/shard_map/all_gather | solution.py:114
  108.9 1.3 multiply_convert_fusion
  110.3 2.4 copy.49
  112.6 1.7 multiply_reduce_fusion.1
  114.6 6.3 %conditional.1 = ((f32[2,1,512]{2,0,1:T(2,128)S(1)}, f32[2,1,512,64]{2,3,0,1:T(8,128)S(1)})) conditional(s32[]{:T(128)} %convert_element_type.124, (f32[2,1,512]{2,0,1:T(2,128)S(1)}, f32[2,1,512,64]{2,3,0,1:T(8,128)S(1)}) %tuple.30, (s32[]{:T(128)}, s32[4,128]{1,0:T(4,128)S(1)}, bf16[2,1,4,128,64]{3,2,4,0,1:T(4,128)(2,1)S(1)}, ...), branch_computations={%region_3.4_spmd, %region_4.7_spmd} | conditional | flops 281680384 | bytes 17967226 | solution.py:160
  114.7 0.8 dynamic-slice_bitcast_fusion
  115.9 2.4 fusion.3
  118.4 1.8 fusion.1
  120.2 0.8 fusion.4
  121.5 1.7 convolution_convert_fusion
  123.3 3.3 %collective-permute-start = (bf16[2,3,256]{2,1,0:T(4,128)(2,1)S(1)}, bf16[2,3,256]{2,1,0:T(4,128)(2,1)S(1)}, u32[]{:S(2)}, u32[]{:S(2)}) collective-permute-start(bf16[2,3,256]{2,1,0:T(4,128)(2,1)S(1)} %slice.399), channel_id=1, source_target_pairs={{0,4},{4,8},{8,12},{12,16},{16,20},{20,24},{24,28},{1,5},{5,9},{9,... | collective-permute-start | bytes 9224 | tf_op jit(solution)/shard_map/ppermute | solution.py:18
  127.2 0.7 collective-permute-done
  129.1 0.8 copy.62
  129.9 1.2 fusion.22
  131.1 0.8 copy.58
  132.0 2.0 convert_multiply_fusion
  134.0 0.7 slice.404
  134.7 1.6 slice.363
  136.4 1.0 slice.317
  137.3 1.6 slice.316
  139.5 0.7 slice.319
  140.2 0.7 slice.315
  140.9 0.7 slice.314
  141.6 1.1 multiply_add_fusion.1
  142.7 0.7 slice.361
  143.5 0.7 slice.320
  147.7 0.8 fusion.53
  148.5 0.6 pad_maximum_fusion.7
  149.2 0.8 pad.128
  151.2 0.7 fusion.49
  151.9 0.9 pad_maximum_fusion.4
  152.8 2.1 pad.116
  154.9 0.8 pad.130
  155.7 1.6 add.383
  157.3 1.7 fusion.45
  159.0 1.5 pad.117
  160.5 2.3 pad.118
  162.8 0.7 slice_add_fusion.4
  163.6 26.3 %all-gather = f32[16,1,256]{2,1,0:T(1,128)S(1)} all-gather(f32[2,1,256]{2,1,0:T(1,128)S(1)} %slice_add_fusion.4), channel_id=2, replica_groups=mesh['sp'=8,'tp'=4] {'sp'}, dimensions={0}, use_global_device_ids=true | all-gather | bytes 18432 | tf_op jit(solution)/shard_map/all_gather | solution.py:201
  190.4 1.6 pad_maximum_fusion.2
  192.0 0.9 pad.131
  193.0 0.6 reduce.15
  193.6 0.7 reshape.378
  194.3 1.2 copy.63
  195.6 1.4 pad.132
  197.0 0.7 slice_add_fusion.3
  197.7 26.1 %all-gather.1 = f32[16,1,256]{2,1,0:T(1,128)S(1)} all-gather(f32[2,1,256]{2,1,0:T(1,128)S(1)} %slice_add_fusion.3), channel_id=3, replica_groups=mesh['sp'=8,'tp'=4] {'sp'}, dimensions={0}, use_global_device_ids=true | all-gather | bytes 18432 | tf_op jit(solution)/shard_map/all_gather | solution.py:200
  224.0 0.7 pad_maximum_fusion.12
  224.9 3.0 %fusion.73 = (f32[2,128,256]{2,1,0:T(8,128)}, f32[2,128,256]{2,1,0:T(8,128)}) fusion(bf16[2,128,2048]{2,1,0:T(8,128)(2,1)} %multiply_convert_fusion, bf16[2048,256]{1,0:T(8,128)(2,1)} %all-gather.10.cloned.1.call-done, f32[2,256]{1,0:T(2,128)S(1)} %fusion.65, f32[2,128,256]{2,1,0:T(8,128)S(1)} %pad.131, f32[2,128,256]{2,1,0:T(8,128)} %pad.132, ...), kind=kOutput, calls=%fused_computation.170 | convolution fusion | flops 269352960 | bytes 3672064 | tf_op jit(solution)/shard_map/dot_general | solution.py:85
  227.9 1.8 copy.64
  229.7 1.2 mul.431
  230.9 1.1 copy.65
  232.1 1.7 fusion.12
  233.8 1.1 copy.94
  234.9 22.5 %reduce-scatter.2.cloned.1.call-done = bf16[256,512]{1,0:T(8,128)(2,1)} async-done(((bf16[1024,512]{1,0:T(8,128)(2,1)}), bf16[256,512]{1,0:T(8,128)(2,1)}) %reduce-scatter.2.cloned.1.call-update) | async-done | bytes 262160 | tf_op jit(solution)/shard_map/reduce_scatter | solution.py:223
  (176 shorter events, 10.7 us)
Async XLA Ops:
  6.5 120.2 %copy-start = (bf16[256,2048]{1,0:T(8,128)(2,1)S(1)}, bf16[256,2048]{1,0:T(8,128)(2,1)}, u32[]{:S(2)}) copy-start(bf16[256,2048]{1,0:T(8,128)(2,1)} %param.38) | copy-start | bytes 3145732
  6.5 70.7 %copy-start.1 = (bf16[2,128,2048]{2,1,0:T(8,128)(2,1)S(1)}, bf16[2,128,2048]{2,1,0:T(8,128)(2,1)}, u32[]{:S(2)}) copy-start(bf16[2,128,2048]{2,1,0:T(8,128)(2,1)} %param.21) | copy-start | bytes 3145732
  6.5 103.7 %all-gather.6.cloned.1.call-start = ((), (), s32[]{:S(2)}) async-start(), calls=%async_computation.1 | async-start | bytes 1179648 | tf_op jit(solution)/shard_map/all_gather | solution.py:77
  7.3 114.3 %all-gather.8.cloned.1.call-start = ((), (), s32[]{:S(2)}) async-start(), calls=%async_computation.2 | async-start | bytes 1179648 | tf_op jit(solution)/shard_map/all_gather | solution.py:80
  8.0 216.8 %all-gather.10.cloned.1.call-start = ((), (), s32[]{:S(2)}) async-start(), calls=%async_computation.3 | async-start | bytes 1179648 | tf_op jit(solution)/shard_map/all_gather | solution.py:81
  8.7 248.6 %reduce-scatter.2.cloned.1.call-start = ((), (), s32[]{:S(2)}) async-start(), calls=%async_computation.4 | async-start | bytes 1310720 | tf_op jit(solution)/shard_map/reduce_scatter | solution.py:223
  77.2 2.0 copy-start.15
  78.2 30.7 %copy-start.8 = (f32[2048]{0:T(1024)S(1)}, f32[2048]{0:T(1024)}, u32[]{:S(2)}) copy-start(f32[2048]{0:T(1024)} %param.22) | copy-start | bytes 24580
  110.2 2.4 copy-start.2
  112.6 1.7 copy-start.16
  115.9 2.5 copy-start.6
  118.3 1.8 copy-start.3
  121.0 5.6 %copy-start.13 = (f32[256]{0:T(256)S(1)}, f32[256]{0:T(256)}, u32[]{:S(2)}) copy-start(f32[256]{0:T(256)} %param.36) | copy-start | bytes 3076
  123.2 4.6 %copy-start.9 = (f32[1,256]{1,0:T(1,128)S(1)}, f32[1,256]{1,0:T(1,128)}, u32[]{:S(2)}) copy-start(f32[1,256]{1,0:T(1,128)} %get-tuple-element.199) | copy-start | bytes 3076
  123.2 4.6 %copy-start.10 = (f32[1,256]{1,0:T(1,128)S(1)}, f32[1,256]{1,0:T(1,128)}, u32[]{:S(2)}) copy-start(f32[1,256]{1,0:T(1,128)} %get-tuple-element.200) | copy-start | bytes 3076
  123.2 4.6 %copy-start.11 = (f32[1,256]{1,0:T(1,128)S(1)}, f32[1,256]{1,0:T(1,128)}, u32[]{:S(2)}) copy-start(f32[1,256]{1,0:T(1,128)} %get-tuple-element.201) | copy-start | bytes 3076
  123.2 4.6 %copy-start.12 = (f32[1,256]{1,0:T(1,128)S(1)}, f32[1,256]{1,0:T(1,128)}, u32[]{:S(2)}) copy-start(f32[1,256]{1,0:T(1,128)} %get-tuple-element.202) | copy-start | bytes 3076
  123.3 4.6 %collective-permute-start = (bf16[2,3,256]{2,1,0:T(4,128)(2,1)S(1)}, bf16[2,3,256]{2,1,0:T(4,128)(2,1)S(1)}, u32[]{:S(2)}, u32[]{:S(2)}) collective-permute-start(bf16[2,3,256]{2,1,0:T(4,128)(2,1)S(1)} %slice.399), channel_id=1, source_target_pairs={{0,4},{4,8},{8,12},{12,16},{16,20},{20,24},{24,28},{1,5},{5,9},{9,... | collective-permute-start | bytes 9224 | tf_op jit(solution)/shard_map/ppermute | solution.py:18
  126.6 2.2 copy-start.17
  128.1 0.7 copy-start.7
  144.1 7.1 %copy-start.4 = (f32[2,31,256]{2,1,0:T(8,128)S(1)}, f32[2,31,256]{2,1,0:T(8,128)}, u32[]{:S(2)}) copy-start(f32[2,31,256]{2,1,0:T(8,128)} %slice.361) | copy-start | bytes 190468
  144.2 7.1 %copy-start.5 = (f32[2,31,256]{2,1,0:T(8,128)S(1)}, f32[2,31,256]{2,1,0:T(8,128)}, u32[]{:S(2)}) copy-start(f32[2,31,256]{2,1,0:T(8,128)} %slice.320) | copy-start | bytes 190468
  224.8 7.1 %copy-start.14 = (f32[256]{0:T(256)S(1)}, f32[256]{0:T(256)}, u32[]{:S(2)}) copy-start(f32[256]{0:T(256)} %param.37) | copy-start | bytes 3076
Sparse Core Ops, SparseCore 0:
  9.5 44.2 all-gather.5
  55.9 41.5 all-gather.7
  99.6 38.9 all-gather.9
  235.0 22.3 reduce-scatter.1
where the time goes:
time: 265 us; the launch traced here: 264 us
  blocking collectives  147 us (55%)
  local copies, waits for them, and re-layouts  35.4 us (13%)
  waiting for transfers between devices  25.4 us (10%)
  other arithmetic  24.8 us (9%)
  matrix products  14.1 us (5%)
  between operations  13.9 us (5%)
  starting transfers between devices  3.38 us (1%)
    all_gather x1, blocking collectives, body(): lax.all_gather(key_weight, 'sp', axis=0, tiled=True)  33.4 us
    all_gather x1, blocking collectives, body(): lax.all_gather(value_weight, 'sp', axis=0, tiled=True)  31.4 us
    all_gather x1, blocking collectives, body(): shard_part = lax.all_gather(key_value, 'sp', axis=1, tiled=True)  29.7 us
    all_gather x1, blocking collectives, body(): lax.all_gather(local_state[:, seq_span - 1][None], 'sp', axis=0, tiled=True)  26.3 us
    all_gather x1, blocking collectives, body(): lax.all_gather(cum_decay[:, seq_span - 1][None], 'sp', axis=0, tiled=True)  26.1 us
    reduce_scatter x1, waiting for transfers between devices, body(): lax.psum_scatter(terms.reshape(row_count, pieces, out_cols).transpose(1,...  22.5 us
    slice x44, local copies, waits for them, and re-layouts, body(): lax.associative_scan(merge_state, (jnp.exp(log_decay), drive), axis=1)  11.2 us
    pad x24, local copies, waits for them, and re-layouts, body(): lax.associative_scan(merge_state, (jnp.exp(log_decay), drive), axis=1)  10.2 us
  transfers between devices with their start and end apart: 5, of which 2 were waited for; matrix products, arithmetic and copies ran while one was open for 24% of the time, Pallas kernels for 0%

commit v1 on v0

v1 whole, which is shorter than its diff:
```python
import functools

import jax
import jax.numpy as jnp
from jax import lax
from jax.experimental import pallas as pl
from jax.experimental.pallas import tpu as pltpu
from jax.sharding import PartitionSpec as P

LRU_CONST = 8.0
EPS = 1e-06
F32 = jnp.float32
BF16 = jnp.bfloat16
MESH = pl.DeviceIdType.MESH


def group_rms(values, gain, width):
    parts = []
    for start in range(0, values.shape[1], width):
        part = values[:, start : start + width]
        scale = lax.rsqrt(jnp.mean(part * part, axis=-1, keepdims=True) + EPS)
        parts.append(part * scale)
    return jnp.concatenate(parts, axis=1) * gain


def one_minus_exp(y):
    series = y * (1 + y / 2 * (1 + y / 3 * (1 + y / 4 * (1 + y / 5 * (1 + y / 6 * (1 + y / 7))))))
    return -jnp.where(y > -0.4, series, jnp.exp(y) - 1.0)


def softplus(x):
    u = jnp.exp(-jnp.abs(x))
    s = u / (2.0 + u)
    q = s * s
    series = 1.0 / 17
    for odd in (15, 13, 11, 9, 7, 5, 3, 1):
        series = series * q + 1.0 / odd
    return jnp.maximum(x, 0.0) + 2.0 * s * series


def sigmoid(x):
    return 1.0 / (1.0 + jnp.exp(-x))


def gelu(x):
    return 0.5 * x * (1.0 + jnp.tanh(0.7978845608028654 * (x + 0.044715 * x * x * x)))


def dot(a, b):
    return jnp.dot(a, b, preferred_element_type=F32)


def kernel(
    dims,
    x_ref, norm_ref, wq_ref, wk_ref, wv_ref, qg_ref, kg_ref, fc_ref, wr_ref, wg_ref, cw_ref,
    dgw_ref, igw_ref, dp_ref, de_ref, ag_ref, rg_ref, oa_ref, or_ref,
    out_ref,
    normed, kvw, rw, qw, gw, kv_all, rin, halo, st_all, halves, sums, parts, got,
    zs, zr, fs, fr, hs, hr, ss, sr, ps, pr, qs, qr,
):
    n, nt, seqs, span, head_dim, block, length = dims
    rows = seqs * span
    no, nto = n // 2, nt // 2
    me = lax.axis_index("sp")
    outer, inner = lax.div(me, 2), lax.rem(me, 2)
    mate = outer * 2 + (1 - inner)
    tme = lax.axis_index("tp")
    touter, tinner = lax.div(tme, 2), lax.rem(tme, 2)
    tmate = touter * 2 + (1 - tinner)
    kr = wq_ref.shape[0]
    kvc = wk_ref.shape[1]
    att_local = wq_ref.shape[1] // head_dim
    kv_local = kvc // head_dim
    hg = att_local // kv_local
    taps = cw_ref.shape[0]

    def to_outer(d):
        return lax.rem(outer + d, no) * 2 + inner

    def from_outer(d):
        return lax.rem(outer + no - d, no) * 2 + inner

    barrier = pltpu.get_barrier_semaphore()
    for d in range(1, n):
        pl.semaphore_signal(barrier, inc=1, device_id={"sp": lax.rem(me + d, n)}, device_id_type=MESH)
    for d in range(1, nt):
        pl.semaphore_signal(barrier, inc=1, device_id={"tp": lax.rem(tme + d, nt)}, device_id_type=MESH)

    def slot(ref, who):
        return ref.at[pl.ds(pl.multiple_of(who * kr, kr), kr), :]

    own_rows = pl.ds(pl.multiple_of(me * kr, kr), kr)
    kvw[own_rows, :] = jnp.concatenate([wk_ref[...], wv_ref[...]], axis=1)
    rw[own_rows, :] = wr_ref[...]
    qw[own_rows, :] = wq_ref[...]
    gw[own_rows, :] = wg_ref[...]
    pl.semaphore_wait(barrier, n - 1 + nt - 1)

    buffers = (kvw, rw, qw, gw, kv_all)
    sources = (None, wr_ref, wq_ref, wg_ref, None)

    def place(c, who):
        return kv_all.at[who] if c == 4 else slot(buffers[c], who)

    def origin(c):
        return place(c, me) if sources[c] is None else sources[c]

    def outward(c, d, who, src):
        return pltpu.make_async_remote_copy(
            src_ref=src, dst_ref=place(c, who), send_sem=zs.at[c, d - 1], recv_sem=zr.at[c, d - 1],
            device_id={"sp": to_outer(d)}, device_id_type=MESH,
        )

    def across(c, d, who, src):
        return pltpu.make_async_remote_copy(
            src_ref=src, dst_ref=place(c, who), send_sem=fs.at[c, d], recv_sem=fr.at[c, d],
            device_id={"sp": mate}, device_id_type=MESH,
        )

    def send_own(c):
        for d in range(1, no):
            outward(c, d, me, origin(c)).start()
        across(c, 0, me, origin(c)).start()

    def forward(c):
        for d in range(1, no):
            who = from_outer(d)
            outward(c, d, who, place(c, who)).wait_recv()
            across(c, d, who, place(c, who)).start()

    def finish(c):
        for d in range(no):
            who = lax.rem(outer + no - d, no) * 2 + (1 - inner)
            across(c, d, who, place(c, who)).wait_recv()

    def drain(c):
        for d in range(1, no):
            outward(c, d, me, origin(c)).wait_send()
        across(c, 0, me, origin(c)).wait_send()
        for d in range(1, no):
            who = from_outer(d)
            across(c, d, who, place(c, who)).wait_send()

    send_own(0)
    send_own(1)
    send_own(2)

    x = x_ref[...].astype(F32)
    scale = lax.rsqrt(jnp.mean(x * x, axis=-1, keepdims=True) + EPS)
    normed[...] = (x * scale * norm_ref[...]).astype(BF16)

    forward(0)
    forward(1)
    finish(0)
    kv = dot(normed[...], kvw[...])
    keys = jnp.concatenate(
        [group_rms(kv[:, g * head_dim : (g + 1) * head_dim], kg_ref[...], head_dim) for g in range(kv_local)], axis=1
    )
    kv_all[me] = jnp.concatenate([keys, kv[:, kvc:]], axis=1).astype(BF16)
    send_own(4)

    finish(1)
    rec = dot(normed[...], rw[...]).astype(BF16).astype(F32)
    nxt, prv = lax.rem(me + 1, n), lax.rem(me + n - 1, n)
    for b in range(seqs):
        rin[b, pl.ds(8, span), :] = rec[b * span : (b + 1) * span]
    for b in range(seqs):
        halo[0, pl.ds(b * 8, 8), :] = rin[b, pl.ds(span, 8), :]
    halo_copy = pltpu.make_async_remote_copy(
        src_ref=halo.at[0], dst_ref=halo.at[1], send_sem=hs, recv_sem=hr,
        device_id={"sp": nxt}, device_id_type=MESH,
    )
    halo_copy.start()
    send_own(3)

    forward(2)
    forward(4)

    halo_copy.wait()
    first = me == 0
    for b in range(seqs):
        edge = halo[1, pl.ds(b * 8, 8), :]
        rin[b, pl.ds(0, 8), :] = jnp.where(first, jnp.zeros_like(edge), edge)
    convs = []
    for b in range(seqs):
        conv = jnp.zeros((span, rw.shape[1]), F32)
        for tap in range(taps):
            conv = conv + rin[b, pl.ds(8 - (taps - 1) + tap, span), :] * cw_ref[pl.ds(tap, 1), :]
        convs.append(conv)
    conv = jnp.concatenate(convs, axis=0).astype(BF16)
    nb, lb = dgw_ref.shape[0], dgw_ref.shape[1]
    gate_decay = jnp.concatenate([dot(conv[:, i * lb : (i + 1) * lb], dgw_ref[i]) for i in range(nb)], axis=1)
    gate_input = jnp.concatenate([dot(conv[:, i * lb : (i + 1) * lb], igw_ref[i]) for i in range(nb)], axis=1)
    log_decay = -LRU_CONST * sigmoid(gate_decay) * softplus(-dp_ref[...]) + de_ref[...]
    state = jnp.sqrt(one_minus_exp(2.0 * log_decay)) * sigmoid(gate_input) * conv.astype(F32)
    decay = jnp.exp(log_decay)
    time = lax.rem(lax.broadcasted_iota(jnp.int32, state.shape, 0), span)
    shift = 1
    while shift < span:
        seen = time >= shift
        state = state + decay * jnp.where(seen, pltpu.roll(state, shift, 0), 0.0)
        decay = decay * jnp.where(seen, pltpu.roll(decay, shift, 0), 1.0)
        shift *= 2
    ends = [decay[(b + 1) * span - 1 : (b + 1) * span] for b in range(seqs)]
    ends += [state[(b + 1) * span - 1 : (b + 1) * span] for b in range(seqs)]
    for i, row in enumerate(ends):
        st_all[me, pl.ds(i, 1), :] = row
    def state_copy(d, who):
        return pltpu.make_async_remote_copy(
            src_ref=st_all.at[who], dst_ref=st_all.at[who], send_sem=ss.at[d - 1], recv_sem=sr.at[d - 1],
            device_id={"sp": lax.rem(me + d, n)}, device_id_type=MESH,
        )

    for d in range(1, n):
        state_copy(d, me).start()

    finish(2)
    scaling = head_dim ** (-0.5)
    query = dot(normed[...], qw[...])
    queries = [
        (group_rms(query[:, h * head_dim : (h + 1) * head_dim], qg_ref[...], head_dim).astype(BF16) * scaling).astype(BF16)
        for h in range(att_local)
    ]
    finish(4)
    shards = block // span
    first_pos = me * span
    query_pos = first_pos + lax.broadcasted_iota(jnp.int32, (span, block), 0)
    key_off = lax.broadcasted_iota(jnp.int32, (span, block), 1)
    needed = lax.div(first_pos + span + block - 1, block)
    attended = []
    for b in range(seqs):
        heads = []
        for h in range(att_local):
            g = h // hg
            q = queries[h][b * span : (b + 1) * span]

            def step(j, carried, q=q, b=b, h=h, g=g):
                top, total, accum = carried
                kvb = kv_all[pl.ds(j * shards, shards), pl.ds(b * span, span), :].reshape(block, 2 * kvc)
                kb = kvb[:, g * head_dim : (g + 1) * head_dim]
                vb = kvb[:, kvc + g * head_dim : kvc + (g + 1) * head_dim]
                s = lax.dot_general(q, kb, (((1,), (1,)), ((), ())), preferred_element_type=F32)
                s = s - fc_ref[b, pl.ds(h, 1), pl.ds(pl.multiple_of(j * block, block), block)]
                s = jnp.where(query_pos >= key_off + j * block, s, -jnp.inf)
                new_top = jnp.maximum(top, jnp.max(s, axis=-1, keepdims=True))
                w = jnp.exp(s - new_top)
                fade = jnp.exp(top - new_top)
                total = total * fade + jnp.sum(w, axis=-1, keepdims=True)
                return new_top, total, accum * fade + dot(w.astype(BF16), vb)

            start = (jnp.full((span, 1), -1e30, F32), jnp.zeros((span, 1), F32), jnp.zeros((span, head_dim), F32))
            if length == block:
                top, total, accum = step(0, start)
            else:
                top, total, accum = lax.fori_loop(0, needed, step, start)
            value = accum / total
            value = value * lax.rsqrt(jnp.mean(value * value, axis=-1, keepdims=True) + EPS)
            heads.append(value)
        attended.append(jnp.concatenate(heads, axis=1))
    halves[0] = (jnp.concatenate(attended, axis=0) * ag_ref[...]).astype(BF16)

    forward(3)
    for d in range(1, n):
        state_copy(d, lax.rem(me + n - d, n)).wait_recv()

    def enter(j, e):
        block_state = st_all[j]
        return block_state[0:seqs] * e + block_state[seqs : 2 * seqs]

    entering = lax.fori_loop(0, me, enter, jnp.zeros((seqs, rw.shape[1]), F32))
    whole_state = jnp.concatenate(
        [
            state[b * span : (b + 1) * span] + decay[b * span : (b + 1) * span] * entering[b : b + 1]
            for b in range(seqs)
        ],
        axis=0,
    )
    finish(3)
    gated = whole_state * gelu(dot(normed[...], gw[...]))
    halves[1] = group_rms(gated, rg_ref[...], lb).astype(BF16)

    cols = out_ref.shape[1]

    def piece(who):
        span_cols = pl.ds(pl.multiple_of(who * cols, cols), cols)
        return dot(halves[0], oa_ref[:, span_cols]) + dot(halves[1], or_ref[:, span_cols])

    def to_mate(s):
        return pltpu.make_async_remote_copy(
            src_ref=sums.at[s], dst_ref=parts.at[s], send_sem=ps.at[s], recv_sem=pr.at[s],
            device_id={"tp": tmate}, device_id_type=MESH,
        )

    def to_far(d):
        return pltpu.make_async_remote_copy(
            src_ref=sums.at[nto + d - 1], dst_ref=got.at[d - 1], send_sem=qs.at[d - 1], recv_sem=qr.at[d - 1],
            device_id={"tp": lax.rem(touter + d, nto) * 2 + tinner}, device_id_type=MESH,
        )

    for s in list(range(1, nto)) + [0]:
        sums[s] = piece(lax.rem(touter + s, nto) * 2 + (1 - tinner)).astype(BF16)
        to_mate(s).start()
    for d in range(1, nto):
        mine = piece(lax.rem(touter + d, nto) * 2 + tinner)
        to_mate(d).wait_recv()
        sums[nto + d - 1] = (mine + parts[d].astype(F32)).astype(BF16)
        to_far(d).start()
    mine = piece(tme)
    to_mate(0).wait_recv()
    mine = mine + parts[0].astype(F32)
    for d in range(1, nto):
        to_far(d).wait_recv()
        mine = mine + got[d - 1].astype(F32)
    out_ref[...] = mine.astype(BF16)

    for c in range(5):
        drain(c)
    for d in range(1, n):
        state_copy(d, me).wait_send()
    for s in range(nto):
        to_mate(s).wait_send()
    for d in range(1, nto):
        to_far(d).wait_send()


def body(
    n, nt,
    inputs, norm_gain, query_weight, key_weight, value_weight, query_gain, key_gain, forget_cache,
    rec_in_weight, rec_gate_weight, conv_weight, decay_gate_weight, input_gate_weight, decay_param,
    decay_extra, attn_out_gain, rec_out_gain, out_att_weight, out_rec_weight,
):
    seqs, span, width = inputs.shape
    rows = seqs * span
    head_dim = query_gain.shape[0]
    length = forget_cache.shape[2]
    channels = rec_in_weight.shape[1]
    qc, kvc = query_weight.shape[1], key_weight.shape[1]
    cols = out_att_weight.shape[1] // nt
    block = span
    while block * 2 <= 1024 and length % (block * 2) == 0:
        block *= 2
    no, nto = n // 2, nt // 2
    dma = pltpu.SemaphoreType.DMA
    vmem = pl.BlockSpec(memory_space=pltpu.VMEM)
    out = pl.pallas_call(
        functools.partial(kernel, (n, nt, seqs, span, head_dim, block, length)),
        out_shape=jax.ShapeDtypeStruct((rows, cols), BF16),
        in_specs=[vmem] * 19,
        out_specs=vmem,
        scratch_shapes=[
            pltpu.VMEM((rows, width), BF16),
            pltpu.VMEM((width, 2 * kvc), BF16),
            pltpu.VMEM((width, channels), BF16),
            pltpu.VMEM((width, qc), BF16),
            pltpu.VMEM((width, channels), BF16),
            pltpu.VMEM((n, rows, 2 * kvc), BF16),
            pltpu.VMEM((seqs, span + 8, channels), F32),
            pltpu.VMEM((2, seqs * 8, channels), F32),
            pltpu.VMEM((n, -(-2 * seqs // 8) * 8, channels), F32),
            pltpu.VMEM((2, rows, channels), BF16),
            pltpu.VMEM((2 * nto, rows, cols), BF16),
            pltpu.VMEM((nto, rows, cols), BF16),
            pltpu.VMEM((nto, rows, cols), BF16),
            dma((5, no)), dma((5, no)), dma((5, no)), dma((5, no)),
            dma, dma, dma((n,)), dma((n,)),
            dma((nto,)), dma((nto,)), dma((nto,)), dma((nto,)),
        ],
        compiler_params=pltpu.CompilerParams(
            collective_id=0, has_side_effects=True, vmem_limit_bytes=60 * 1024 * 1024
        ),
    )(
        inputs.reshape(rows, width), norm_gain.reshape(1, width), query_weight, key_weight, value_weight,
        query_gain.reshape(1, head_dim), key_gain.reshape(1, head_dim), forget_cache,
        rec_in_weight, rec_gate_weight, conv_weight.astype(F32), decay_gate_weight, input_gate_weight,
        decay_param.reshape(1, channels), decay_extra.reshape(rows, channels),
        attn_out_gain.reshape(1, qc), rec_out_gain.reshape(1, channels), out_att_weight, out_rec_weight,
    )
    return out.reshape(seqs, span, cols)


def solution(mesh):
    return jax.shard_map(
        functools.partial(body, mesh.shape["sp"], mesh.shape["tp"]),
        mesh=mesh,
        in_specs=(
            P(None, "sp", None), P(), P("sp", "tp"), P("sp", "tp"), P("sp", "tp"), P(), P(),
            P(None, "tp", None), P("sp", "tp"), P("sp", "tp"), P(None, "tp"), P("tp", None, None),
            P("tp", None, None), P("tp"), P(None, "sp", "tp"), P("tp"), P("tp"), P("tp", None), P("tp", None),
        ),
        out_specs=P(None, "sp", "tp"),
        check_vma=False,
    )
```

time: 265 us -> 84.6 us (0.32)
  blocking collectives: 147 us -> 0 us
  Pallas kernels: 0 us -> 79.2 us
  local copies, waits for them, and re-layouts: 35.4 us -> 4.59 us
  waiting for transfers between devices: 25.4 us -> 0 us
  other arithmetic: 24.8 us -> 0.59 us
  matrix products: 14.1 us -> 0 us
  between operations: 13.9 us -> 0.01 us
  starting transfers between devices: 3.38 us -> 0 us
    all_gather x5 -> x0, blocking collectives: 147 us -> none  [the longest x1 33.4 us: body(): lax.all_gather(key_weight, 'sp', axis=0, tiled=True)]
    pallas_call x0 -> x1, Pallas kernels: none -> 79.2 us  [body(): pl.pallas_call(functools.partial(kernel, (n, nt, seqs, span, head_dim, bl...]
    reduce_scatter x1 -> x0, waiting for transfers between devices: 22.5 us -> none  [body(): lax.psum_scatter(terms.reshape(row_count, pieces, out_cols).transpose(1,...]
    dot_general x11 -> x0, matrix products: 14.1 us -> none  [the longest x5 7.32 us: body(): lax.dot_general(normed_cols, weight_part, row_contract, preferred_element...]
    slice x47 -> x0, local copies, waits for them, and re-layouts: 13 us -> none  [the longest x44 11.2 us: body(): lax.associative_scan(merge_state, (jnp.exp(log_decay), drive), axis=1)]
    pad x28 -> x0, local copies, waits for them, and re-layouts: 10.3 us -> none  [the longest x24 10.2 us: body(): lax.associative_scan(merge_state, (jnp.exp(log_decay), drive), axis=1)]
    add x29 -> x0, other arithmetic: 9.33 us -> none  [the longest x13 4.97 us: body(): lax.associative_scan(merge_state, (jnp.exp(log_decay), drive), axis=1)]
    convert_element_type x8 -> x1, other arithmetic: 5.91 us -> 0.59 us  [body(): conv_weight.astype(F32)]
  transfers between devices with their start and end apart: 5 -> 0, of which waited for: 2 -> 0; matrix products, arithmetic and copies ran while one was open for 24% -> 0% of each run, Pallas kernels for 0% -> 0%
where the time goes in v1:
time: 84.6 us; the launch traced here: 84.4 us
  Pallas kernels  79.2 us (94%)
  local copies, waits for them, and re-layouts  4.59 us (5%)
    pallas_call x1, Pallas kernels, body(): pl.pallas_call(functools.partial(kernel, (n, nt, seqs, span, head_dim, bl...  79.2 us
    unnamed x7, local copies, waits for them, and re-layouts  4.59 us

profile of v1, /device:TPU:0, one launch (start us, length us, event | category | flops | bytes accessed | tf_op | source)
XLA Modules:
  0.0 84.4 jit_solution(5291823098604318668)
XLA Ops:
  0.0 0.0 copy-start.1
  0.0 0.7 copy-done.1
  0.7 0.6 convert_element_type.3.cw_ref
  1.3 0.0 copy-start
  1.3 1.5 %copy.20.wk_ref = bf16[256,64]{1,0:T(8,128)(2,1)} copy(bf16[256,64]{0,1:T(8,128)(2,1)} %param.22) | data formatting | bytes 65536 | tf_op args[3]
  2.8 0.0 copy-done
  2.8 0.7 copy.21.wv_ref
  3.5 79.2 %shard_map.181 = bf16[256,512]{1,0:T(8,128)(2,1)} custom-call(bf16[256,2048]{1,0:T(8,128)(2,1)} %bitcast.10, f32[1,2048]{1,0:T(1,128)} %bitcast.12, bf16[256,256]{1,0:T(8,128)(2,1)} %wq_ref.1, bf16[256,64]{1,0:T(8,128)(2,1)} %copy.20.wk_ref, bf16[256,64]{1,0:T(8,128)(2,1)} %copy.21.wv_ref, f32[1,64]{1,0:T(1,128)} %bitcast.16, f32[1,64]{1,0:T(1,128)} %bitcast.17, ...), custom_call_target="tpu_custom_call" | custom-call | tf_op jit(solution)/shard_map/pallas_call | solution.py:345
  82.7 1.7 %copy.23 = bf16[2,128,512]{2,1,0:T(8,128)(2,1)} copy(bf16[2,128,512]{2,1,0:T(8,128)(2,1)} %bitcast.9) | data formatting | bytes 524288
Async XLA Ops:
  0.0 0.7 copy-start.1
  1.3 1.5 %copy-start = (bf16[256,64]{0,1:T(8,128)(2,1)S(1)}, bf16[256,64]{0,1:T(8,128)(2,1)}, u32[]{:S(2)}) copy-start(bf16[256,64]{0,1:T(8,128)(2,1)} %param.23) | copy-start | bytes 98308
